TPU v7x, 32 devices: a whole 2x2x4 slice. The times are simulated.
32 devices in a mesh: sp: 4 (over z), dp: 8 (over y, x, core).
Axes of the slice: x: 2, y: 2, z: 4, core: 2. Of those that a mesh axis runs over, the one named last changes fastest.
Arguments:
- cotangent: bfloat16 [8, 512, 2048], P('dp', 'sp'), may hold values from -6 to 6
- unit_pre: bfloat16 [8, 512, 2048], P('dp', None, 'sp'), may hold values from -6 to 6
- gate_pre: bfloat16 [8, 512, 2048], P('dp', None, 'sp'), may hold values from -15 to 15
- out_weight: bfloat16 [2048, 2048], P('dp', 'sp'), may hold values from -0.125 to 0.125
- mix_weight: bfloat16 [8, 128, 128], replicated, may hold values from -0.5 to 0.5
- mix_bias: bfloat16 [8, 128], replicated, may hold values from 0.099609375 to 1.8984375
- norm_gain: bfloat16 [2048], P('sp'), may hold values from 0.099609375 to 1.8984375
- norm_shift: bfloat16 [2048], P('sp'), may hold values from -3 to 3
Outputs:
- unit_grad: bfloat16 [8, 512, 2048], P('dp', None, 'sp')
- gate_grad: bfloat16 [8, 512, 2048], P('dp', None, 'sp')
- out_weight_grad: float32 [2048, 2048], P('dp', 'sp')
- mix_weight_grad: float32 [8, 128, 128], replicated
- mix_bias_grad: float32 [8, 128], replicated
- gain_grad: float32 [2048], P('sp')
- shift_grad: float32 [2048], P('sp')
All inputs are finite; a program needn't handle non-finite values.
Results may differ from a plain program's by a relative error of at most 0.015.
Values may be sent and summed in bfloat16 or wider, within the bound.
No kernel may reach another device: no remote copies, remote signals or barrier semaphores. Data moves between devices by JAX's collectives and lax.ppermute only.
A program may use at most 64 MiB of HBM per device.

v0:
```python
import math
import jax
import jax.numpy as jnp
from jax import lax
from jax.sharding import PartitionSpec as P

GW = 2048
GROUPS = 8
BLK = 128
epsilon = 1e-05
tanh_coef = math.sqrt(2.0 / math.pi)


def gelu_slope(values):
    inner = tanh_coef * (values + 0.044715 * values * values * values)
    hyper = jnp.tanh(inner)
    return 0.5 * (1.0 + hyper) + 0.5 * values * (1.0 - hyper * hyper) * tanh_coef * (
        1.0 + 3.0 * 0.044715 * values * values
    )


def local(cotangent, unit_pre, gate_pre, out_weight, mix_weight, mix_bias, norm_gain, norm_shift):
    seq_len = unit_pre.shape[1]
    channels = unit_pre.shape[2]
    group_dim = GW // GROUPS
    span_width = min(channels, group_dim)
    groups_here = channels // span_width
    blocks = seq_len // BLK
    group_start = lax.axis_index("sp") * channels // group_dim
    units = unit_pre[0].astype(jnp.float32)
    gates = gate_pre[0].astype(jnp.float32)
    unit_act = jax.nn.gelu(units)
    gate_act = jax.nn.gelu(gates)
    moments = lax.psum((jnp.sum(gate_act, axis=-1), jnp.sum(gate_act * gate_act, axis=-1)), "sp")
    mean_val = moments[0] / GW
    var_val = moments[1] / GW - mean_val * mean_val
    rstd_val = lax.rsqrt(var_val + epsilon)
    centred = (gate_act - mean_val[:, None]) * rstd_val[:, None]
    gain_vec = norm_gain.astype(jnp.float32)
    normed = (centred * gain_vec + norm_shift.astype(jnp.float32)).astype(jnp.bfloat16)
    causal = jnp.arange(BLK)[:, None] >= jnp.arange(BLK)[None, :]
    local_weight = lax.dynamic_slice_in_dim(mix_weight, group_start, groups_here, 0)
    masked = jnp.where(causal[None], local_weight, jnp.zeros_like(local_weight))
    local_bias = lax.dynamic_slice_in_dim(mix_bias, group_start, groups_here, 0).astype(jnp.float32)
    normed_blocks = normed.reshape(blocks, BLK, groups_here, span_width)
    mixed = jnp.einsum("gts,nsgd->ntgd", masked, normed_blocks, preferred_element_type=jnp.float32)
    mixed = (mixed + local_bias.T[None, :, :, None]).reshape(seq_len, channels)
    gated = (unit_act * mixed).astype(jnp.bfloat16)
    weight_whole = lax.all_gather(out_weight, "dp", axis=0, tiled=True)
    dy_rows = lax.all_gather(cotangent, "sp", axis=1, tiled=True)[0]
    product = jnp.dot(dy_rows, weight_whole, preferred_element_type=jnp.float32)
    weight_part = lax.dot_general(
        dy_rows, gated, (((0,), (0,)), ((), ())), preferred_element_type=jnp.float32
    )
    token_count = lax.axis_size("dp") * seq_len
    norm_scale = 1.0 / math.sqrt(token_count)
    mix_scale = 1.0 / math.sqrt(token_count // BLK * group_dim)
    out_grad = (
        lax.psum_scatter(
            weight_part.astype(jnp.bfloat16), "dp", scatter_dimension=0, tiled=True
        ).astype(jnp.float32)
        * norm_scale
    )
    unit_grad = (product * mixed * gelu_slope(units)).astype(jnp.bfloat16)
    mix_grad = product * unit_act
    mix_round = mix_grad.astype(jnp.bfloat16).reshape(blocks, BLK, groups_here, span_width)
    mix_term = jnp.einsum(
        "ntgd,nsgd->gts", mix_round, normed_blocks, preferred_element_type=jnp.float32
    )
    mix_term = jnp.where(causal[None], mix_term, jnp.float32(0.0))
    bias_term = jnp.sum(mix_grad.reshape(blocks, BLK, groups_here, span_width), axis=(0, 3)).T
    normed_grad = jnp.einsum(
        "gts,ntgd->nsgd", masked, mix_round, preferred_element_type=jnp.float32
    ).reshape(seq_len, channels)
    gain_term = jnp.sum(normed_grad * centred, axis=0)
    shift_term = jnp.sum(normed_grad, axis=0)
    scaled = normed_grad * gain_vec
    back_sums = lax.psum((jnp.sum(scaled, axis=-1), jnp.sum(scaled * centred, axis=-1)), "sp")
    first_m = back_sums[0] / GW
    second_m = back_sums[1] / GW
    gate_grad = (
        rstd_val[:, None]
        * (scaled - first_m[:, None] - centred * second_m[:, None])
        * gelu_slope(gates)
    ).astype(jnp.bfloat16)
    empty_weight = jnp.zeros((GROUPS, BLK, BLK), jnp.float32)
    empty_bias = jnp.zeros((GROUPS, BLK), jnp.float32)
    mix_local, bias_local, gain_total, shift_total = (
        lax.psum(mix_term.astype(jnp.bfloat16), "dp").astype(jnp.float32),
        lax.psum(bias_term.astype(jnp.bfloat16), "dp").astype(jnp.float32),
        lax.psum(gain_term.astype(jnp.bfloat16), "dp").astype(jnp.float32),
        lax.psum(shift_term.astype(jnp.bfloat16), "dp").astype(jnp.float32),
    )
    full_weight = lax.dynamic_update_slice_in_dim(empty_weight, mix_local, group_start, 0)
    full_bias = lax.dynamic_update_slice_in_dim(empty_bias, bias_local, group_start, 0)
    full_weight, full_bias = (
        lax.psum(full_weight.astype(jnp.bfloat16), "sp").astype(jnp.float32),
        lax.psum(full_bias.astype(jnp.bfloat16), "sp").astype(jnp.float32),
    )
    return (
        unit_grad[None],
        gate_grad[None],
        out_grad,
        full_weight * mix_scale,
        full_bias * mix_scale,
        gain_total * norm_scale,
        shift_total * norm_scale,
    )


def solution(mesh):
    in_specs = (
        P("dp", "sp", None),
        P("dp", None, "sp"),
        P("dp", None, "sp"),
        P("dp", "sp"),
        P(),
        P(),
        P("sp"),
        P("sp"),
    )
    out_specs = (
        P("dp", None, "sp"),
        P("dp", None, "sp"),
        P("dp", "sp"),
        P(),
        P(),
        P("sp"),
        P("sp"),
    )
    return jax.shard_map(local, mesh=mesh, in_specs=in_specs, out_specs=out_specs, check_vma=False)
```

profile of v0, /device:TPU:0, one launch (start us, length us, event | category | flops | bytes accessed | tf_op | source)
XLA Modules:
  0.0 237.9 jit_solution(5552104702866696244)
XLA Ops:
  8.7 1.7 reshape.181
  11.7 1.3 copy.78
  13.5 13.9 %all-reduce.1 = (f32[512]{0:T(512)S(1)}, f32[512]{0:T(512)S(1)}) all-reduce(f32[512]{0:T(512)S(1)} %get-tuple-element.40, f32[512]{0:T(512)S(1)} %get-tuple-element.39), channel_id=1, replica_groups=mesh['sp'=4,'dp'=8] {'sp'}, use_global_device_ids=true, to_apply=%region_3.4 | all-reduce | flops 1024 | bytes 8192 | tf_op jit(solution)/shard_map/psum | solution.py:34
  28.2 3.3 %fusion.43 = (bf16[4,128,2,256]{1,3,0,2:T(8,128)(2,1)}, f32[4,128,2,256]{1,3,0,2:T(8,128)}) fusion(f32[4,128,2,256]{1,3,0,2:T(8,128)} %copy.78, f32[128,2]{0,1:T(2,128)S(1)} %convert_bitcast_fusion.1, bf16[8,128,128]{2,1,0:T(8,128)(2,1)S(1)} %copy-done.7, s32[]{:T(128)S(6)} %select_n.20, pred[128,128]{1,0:T(8,128)(4,1)S(1)} %iota_compare_fusion, ...), kind=kOutput, calls=%fused_computation.64 | convolution fusion | flops 73433088 | bytes 3761156 | tf_op jit(solution)/shard_map/gts,nsgd->ntgd/dot_general | solution.py:46
  31.5 1.5 copy.71
  33.0 1.0 copy.87
  34.1 24.0 %all-gather.3.cloned.1.call-done = bf16[1,512,2048]{2,1,0:T(8,128)(2,1)} async-done(((bf16[1,128,2048]{2,1,0:T(8,128)(2,1)}), bf16[1,512,2048]{2,1,0:T(8,128)(2,1)}) %all-gather.3.cloned.1.call-update) | async-done | bytes 2097168 | tf_op jit(solution)/shard_map/all_gather | solution.py:50
  58.0 28.5 %all-gather.5.cloned.1.call-done = bf16[2048,512]{1,0:T(8,128)(2,1)} async-done(((bf16[256,512]{1,0:T(8,128)(2,1)}), bf16[2048,512]{1,0:T(8,128)(2,1)}) %all-gather.5.cloned.1.call-update) | async-done | bytes 2097168 | tf_op jit(solution)/shard_map/all_gather | solution.py:49
  86.6 5.6 %fusion.85 = (bf16[512,512]{1,0:T(8,128)(2,1)}, f32[512,512]{1,0:T(8,128)S(1)}, bf16[1,512,512]{2,1,0:T(8,128)(2,1)}) fusion(bf16[1,512,512]{2,1,0:T(8,128)(2,1)S(1)} %copy-done.2, f32[512,512]{1,0:T(8,128)} %bitcast.107, bf16[2048,512]{1,0:T(8,128)(2,1)} %all-gather.5.cloned.1.call-done, bf16[1,512,2048]{2,1,0:T(8,128)(2,1)} %all-gather.3.cloned.1.call-done), kind=kOutput, calls=%fused_computation.126 | convolution fusion | flops 1081868288 | bytes 7864320 | tf_op jit(solution)/shard_map/dot_general | solution.py:51
  92.2 1.2 reshape.178
  93.3 1.4 fusion.10
  94.8 1.4 copy.79
  97.1 51.0 %all-reduce.6.cloned.1.call-done = bf16[2,128,128]{2,1,0:T(8,128)(2,1)} async-done(((bf16[2,128,128]{2,1,0:T(8,128)(2,1)}), bf16[2,128,128]{2,1,0:T(8,128)(2,1)}) %all-reduce.6.cloned.1.call-update) | async-done | bytes 65552 | tf_op jit(solution)/shard_map/psum | solution.py:89
  149.7 4.3 %fusion = bf16[2048,512]{0,1:T(8,128)(2,1)} fusion(bf16[512,512]{1,0:T(8,128)(2,1)} %bitcast.108, bf16[1,512,2048]{2,1,0:T(8,128)(2,1)} %all-gather.3.cloned.1.call-done), kind=kOutput, calls=%fused_computation.13 | convolution fusion | flops 1074790400 | bytes 4718592 | tf_op jit(solution)/shard_map/dot_general | solution.py:52
  154.1 1.0 copy-done.4
  155.1 1.8 multiply_reduce_fusion
  158.1 1.6 copy.73
  160.5 11.8 %all-reduce.2 = (bf16[2,128]{1,0:T(2,128)(2,1)S(1)}, bf16[512]{0:T(512)(128)(2,1)S(1)}, bf16[512]{0:T(512)(128)(2,1)S(1)}) all-reduce(bf16[2,128]{1,0:T(2,128)(2,1)S(1)} %bitcast.114, bf16[512]{0:T(512)(128)(2,1)S(1)} %bitcast.112, bf16[512]{0:T(512)(128)(2,1)S(1)} %bitcast.113), channel_id=1, replica_groups=mesh['sp'=4,'dp'=8] {'dp'}, use_global_device_ids=true, to_apply=%region_12.13 | all-reduce | flops 1280 | bytes 5120 | tf_op jit(solution)/shard_map/psum | solution.py:90
  172.4 12.0 %psum.77 = bf16[8,128]{1,0:T(8,128)(2,1)S(1)} all-reduce(bf16[8,128]{1,0:T(8,128)(2,1)S(1)} %dynamic_update_slice.7), channel_id=1, replica_groups=mesh['sp'=4,'dp'=8] {'sp'}, use_global_device_ids=true, to_apply=%region_13.14 | all-reduce | flops 1024 | bytes 4096 | tf_op jit(solution)/shard_map/psum | solution.py:98
  184.4 8.4 %all-reduce = (f32[512]{0:T(512)S(1)}, f32[512]{0:T(512)S(1)}) all-reduce(f32[512]{0:T(512)S(1)} %bitcast.115, f32[512]{0:T(512)S(1)} %bitcast.116), channel_id=1, replica_groups=mesh['sp'=4,'dp'=8] {'sp'}, use_global_device_ids=true, to_apply=%region_7.8 | all-reduce | flops 1024 | bytes 8192 | tf_op jit(solution)/shard_map/psum | solution.py:78
  193.9 2.1 fusion.69
  196.1 1.8 convert_multiply_fusion.9
  197.9 31.5 %reduce-scatter.2.cloned.1.call-done = bf16[256,512]{0,1:T(8,128)(2,1)} async-done(((bf16[2048,512]{0,1:T(8,128)(2,1)}), bf16[256,512]{0,1:T(8,128)(2,1)}) %reduce-scatter.2.cloned.1.call-update) | async-done | bytes 262160 | tf_op jit(solution)/shard_map/reduce_scatter | solution.py:59
  230.4 1.0 copy.83
  (50 shorter events, 10.8 us)
Async XLA Ops:
  7.2 50.9 %all-gather.3.cloned.1.call-start = ((), (), s32[]{:S(2)}) async-start(), calls=%async_computation.1 | async-start | bytes 2621440 | tf_op jit(solution)/shard_map/all_gather | solution.py:50
  7.9 3.0 %copy-start.5 = (bf16[512]{0:T(512)(128)(2,1)S(1)}, bf16[512]{0:T(512)(128)(2,1)}, u32[]{:S(2)}) copy-start(bf16[512]{0:T(512)(128)(2,1)} %param.14) | copy-start | bytes 3076
  7.9 3.1 %copy-start.6 = (bf16[512]{0:T(512)(128)(2,1)S(1)}, bf16[512]{0:T(512)(128)(2,1)}, u32[]{:S(2)}) copy-start(bf16[512]{0:T(512)(128)(2,1)} %param.15) | copy-start | bytes 3076
  7.9 3.1 %copy-start.2 = (bf16[1,512,512]{2,1,0:T(8,128)(2,1)S(1)}, bf16[1,512,512]{2,1,0:T(8,128)(2,1)}, u32[]{:S(2)}) copy-start(bf16[1,512,512]{2,1,0:T(8,128)(2,1)} %param.9) | copy-start | bytes 1572868
  7.9 78.7 %all-gather.5.cloned.1.call-start = ((), (), s32[]{:S(2)}) async-start(), calls=%async_computation.2 | async-start | bytes 2359296 | tf_op jit(solution)/shard_map/all_gather | solution.py:49
  8.7 139.4 %all-reduce.6.cloned.1.call-start = ((), (), s32[]{:S(2)}) async-start(), calls=%async_computation.4 | async-start | bytes 131072 | tf_op jit(solution)/shard_map/psum | solution.py:89
  11.0 2.0 copy-start
  11.0 17.2 %copy-start.7 = (bf16[8,128,128]{2,1,0:T(8,128)(2,1)S(1)}, bf16[8,128,128]{2,1,0:T(8,128)(2,1)}, u32[]{:S(2)}) copy-start(bf16[8,128,128]{2,1,0:T(8,128)(2,1)} %param.12) | copy-start | bytes 786436
  93.3 1.4 copy-start.3
  94.7 101.3 %all-reduce.8.cloned.1.call-start = ((), (), s32[]{:S(2)}) async-start(), calls=%async_computation.5 | async-start | bytes 524288 | tf_op jit(solution)/shard_map/psum | solution.py:97
  149.0 0.7 copy-start.1
  149.7 79.7 %reduce-scatter.2.cloned.1.call-start = ((), (), s32[]{:S(2)}) async-start(), calls=%async_computation.3 | async-start | bytes 2359296 | tf_op jit(solution)/shard_map/reduce_scatter | solution.py:59
  154.1 1.1 copy-start.4
Sparse Core Ops, SparseCore 0:
  9.5 48.4 all-gather.2
  59.9 26.6 all-gather.4
  94.9 53.1 all-reduce.5
  150.3 35.0 all-reduce.7
  188.4 40.9 reduce-scatter.1
where the time goes:
time: 238 us
  waiting for transfers between devices  136 us (57%)
  blocking collectives  46.1 us (19%)
  matrix products  16.3 us (7%)
  local copies, waits for them, and re-layouts  16.2 us (7%)
  between operations  14 us (6%)
  other arithmetic  8.61 us (4%)
    psum x1, waiting for transfers between devices, local(): lax.psum(mix_term.astype(jnp.bfloat16), 'dp').astype(jnp.float32)  51 us
    reduce_scatter x1, waiting for transfers between devices, local(): lax.psum_scatter(weight_part.astype(jnp.bfloat16), 'dp', scatter_dimensio...  31.5 us
    all_gather x1, waiting for transfers between devices, local(): weight_whole = lax.all_gather(out_weight, 'dp', axis=0, tiled=True)  28.5 us
    all_gather x1, waiting for transfers between devices, local(): dy_rows = lax.all_gather(cotangent, 'sp', axis=1, tiled=True)[0]  24 us
    psum x1, blocking collectives, local(): lax.psum((jnp.sum(gate_act, axis=-1), jnp.sum(gate_act * gate_act, axis=-...  13.9 us
    psum x1, blocking collectives, local(): lax.psum(full_bias.astype(jnp.bfloat16), 'sp').astype(jnp.float32)  12 us
    psum x1, blocking collectives, local(): lax.psum(bias_term.astype(jnp.bfloat16), 'dp').astype(jnp.float32)  11.8 us
    psum x1, blocking collectives, local(): lax.psum((jnp.sum(scaled, axis=-1), jnp.sum(scaled * centred, axis=-1)),...  8.36 us
  transfers between devices with their start and end apart: 5, of which 4 were waited for; matrix products, arithmetic and copies ran while one was open for 12% of the time, Pallas kernels for 0%

commit v1 on v0

--- a/solution.py
+++ b/solution.py
@@ -47,7 +47,9 @@
     mixed = (mixed + local_bias.T[None, :, :, None]).reshape(seq_len, channels)
     gated = (unit_act * mixed).astype(jnp.bfloat16)
     weight_whole = lax.all_gather(out_weight, "dp", axis=0, tiled=True)
-    dy_rows = lax.all_gather(cotangent, "sp", axis=1, tiled=True)[0]
+    dy_rows = jnp.concatenate(
+        lax.all_to_all(jnp.stack([cotangent] * lax.axis_size("sp")), "sp", 0, 0), axis=1
+    )[0]
     product = jnp.dot(dy_rows, weight_whole, preferred_element_type=jnp.float32)
     weight_part = lax.dot_general(
         dy_rows, gated, (((0,), (0,)), ((), ())), preferred_element_type=jnp.float32

time: 238 us -> 226 us (0.950)
  waiting for transfers between devices: 136 us -> 93 us
  blocking collectives: 46.1 us -> 68.5 us
  starting transfers between devices: 0.2 us -> 6.64 us
    all_gather x1, waiting for transfers between devices: 28.5 us -> 0.01 us  [local(): weight_whole = lax.all_gather(out_weight, 'dp', axis=0, tiled=True)]
    all_gather x1 -> x0, waiting for transfers between devices: 24 us -> none  [local(): dy_rows = lax.all_gather(cotangent, 'sp', axis=1, tiled=True)[0]]
    psum x1, blocking collectives: 13.9 us -> 36.2 us  [local(): lax.psum((jnp.sum(gate_act, axis=-1), jnp.sum(gate_act * gate_act, axis=-...]
    psum x1, waiting for transfers between devices: 51 us -> 58.9 us  [local(): lax.psum(mix_term.astype(jnp.bfloat16), 'dp').astype(jnp.float32)]
    all_to_all x0 -> x1, starting transfers between devices: none -> 6.48 us  [local(): lax.all_to_all(jnp.stack([cotangent] * lax.axis_size('sp')), 'sp', 0, 0)]
    another operation x0 -> x1, local copies, waits for them, and re-layouts: none -> 2.63 us  [local(): jnp.stack([cotangent] * lax.axis_size('sp'))]
  transfers between devices with their start and end apart: 5 -> 5, of which waited for: 4 -> 3; matrix products, arithmetic and copies ran while one was open for 12% -> 13% of each run, Pallas kernels for 0% -> 0%
where the time goes in v1:
time: 226 us; the launch traced here: 225 us
  waiting for transfers between devices  93 us (41%)
  blocking collectives  68.5 us (30%)
  local copies, waits for them, and re-layouts  17.8 us (8%)
  matrix products  16.3 us (7%)
  between operations  14 us (6%)
  other arithmetic  8.59 us (4%)
  starting transfers between devices  6.64 us (3%)
    psum x1, waiting for transfers between devices, local(): lax.psum(mix_term.astype(jnp.bfloat16), 'dp').astype(jnp.float32)  58.9 us
    psum x1, blocking collectives, local(): lax.psum((jnp.sum(gate_act, axis=-1), jnp.sum(gate_act * gate_act, axis=-...  36.2 us
    reduce_scatter x1, waiting for transfers between devices, local(): lax.psum_scatter(weight_part.astype(jnp.bfloat16), 'dp', scatter_dimensio...  31.6 us
    psum x1, blocking collectives, local(): lax.psum(full_bias.astype(jnp.bfloat16), 'sp').astype(jnp.float32)  12.1 us
    psum x1, blocking collectives, local(): lax.psum(bias_term.astype(jnp.bfloat16), 'dp').astype(jnp.float32)  11.8 us
    psum x1, blocking collectives, local(): lax.psum((jnp.sum(scaled, axis=-1), jnp.sum(scaled * centred, axis=-1)),...  8.36 us
    all_to_all x1, starting transfers between devices, local(): lax.all_to_all(jnp.stack([cotangent] * lax.axis_size('sp')), 'sp', 0, 0)  6.48 us
    dot_general x1, matrix products, local(): product = jnp.dot(dy_rows, weight_whole, preferred_element_type=jnp.float32)  5.57 us
  transfers between devices with their start and end apart: 5, of which 3 were waited for; matrix products, arithmetic and copies ran while one was open for 13% of the time, Pallas kernels for 0%

profile of v1, /device:TPU:0, one launch (start us, length us, event | category | flops | bytes accessed | tf_op | source)
XLA Modules:
  0.0 224.9 jit_solution(8193740500244698372)
XLA Ops:
  7.9 2.6 %stack.2 = bf16[4,1,128,2048]{3,2,1,0:T(8,128)(2,1)} broadcast(bf16[128,2048]{1,0:T(8,128)(2,1)} %bitcast.105), dimensions={2,3} | broadcast | bytes 2621440 | tf_op jit(solution)/shard_map/stack | solution.py:51
  10.5 6.5 %all-to-all-start = ((bf16[4,1,128,2048]{3,2,1,0:T(8,128)(2,1)}), bf16[4,1,128,2048]{3,2,1,0:T(8,128)(2,1)}, u32[]{:S(2)}, u32[]{:S(2)}) async-start(bf16[4,1,128,2048]{3,2,1,0:T(8,128)(2,1)} %stack.2), calls=%async_computation | async-start | bytes 4194304 | tf_op jit(solution)/shard_map/all_to_all | solution.py:51
  19.0 1.3 copy.78
  20.8 36.2 %all-reduce.1 = (f32[512]{0:T(512)S(1)}, f32[512]{0:T(512)S(1)}) all-reduce(f32[512]{0:T(512)S(1)} %get-tuple-element.40, f32[512]{0:T(512)S(1)} %get-tuple-element.39), channel_id=1, replica_groups=mesh['sp'=4,'dp'=8] {'sp'}, use_global_device_ids=true, to_apply=%region_3.4 | all-reduce | flops 1024 | bytes 8192 | tf_op jit(solution)/shard_map/psum | solution.py:34
  57.8 3.3 %fusion.40 = (bf16[4,128,2,256]{1,3,0,2:T(8,128)(2,1)}, f32[4,128,2,256]{1,3,0,2:T(8,128)}) fusion(f32[4,128,2,256]{1,3,0,2:T(8,128)} %copy.78, f32[128,2]{0,1:T(2,128)S(1)} %convert_bitcast_fusion.1, bf16[8,128,128]{2,1,0:T(8,128)(2,1)S(1)} %copy-done.7, s32[]{:T(128)S(6)} %select_n.20, pred[128,128]{1,0:T(8,128)(4,1)S(1)} %iota_compare_fusion, ...), kind=kOutput, calls=%fused_computation.61 | convolution fusion | flops 73433088 | bytes 3761156 | tf_op jit(solution)/shard_map/gts,nsgd->ntgd/dot_general | solution.py:46
  61.1 1.5 copy.71
  62.6 1.1 copy.87
  63.7 1.8 all-to-all-done
  65.5 5.6 %fusion.82 = (bf16[512,512]{1,0:T(8,128)(2,1)}, f32[512,512]{1,0:T(8,128)S(1)}, bf16[1,512,512]{2,1,0:T(8,128)(2,1)}) fusion(bf16[1,512,512]{2,1,0:T(8,128)(2,1)S(1)} %copy-done.2, f32[512,512]{1,0:T(8,128)} %bitcast.104, bf16[512,2048]{1,0:T(8,128)(2,1)} %bitcast.1, bf16[2048,512]{1,0:T(8,128)(2,1)} %all-gather.2.cloned.1.call-done), kind=kOutput, calls=%fused_computation.123 | convolution fusion | flops 1081868288 | bytes 7864320 | tf_op jit(solution)/shard_map/dot_general | solution.py:53
  71.1 1.2 reshape.181
  72.3 1.4 fusion.7
  73.7 1.4 copy.79
  76.0 58.9 %all-reduce.6.cloned.1.call-done = bf16[2,128,128]{2,1,0:T(8,128)(2,1)} async-done(((bf16[2,128,128]{2,1,0:T(8,128)(2,1)}), bf16[2,128,128]{2,1,0:T(8,128)(2,1)}) %all-reduce.6.cloned.1.call-update) | async-done | bytes 65552 | tf_op jit(solution)/shard_map/psum | solution.py:91
  136.5 4.3 %fusion = bf16[2048,512]{0,1:T(8,128)(2,1)} fusion(bf16[512,512]{1,0:T(8,128)(2,1)} %bitcast.106, bf16[512,2048]{1,0:T(8,128)(2,1)} %bitcast.1), kind=kOutput, calls=%fused_computation.13 | convolution fusion | flops 1074790400 | bytes 4718592 | tf_op jit(solution)/shard_map/dot_general | solution.py:54
  140.9 1.0 copy-done.4
  141.9 1.8 multiply_reduce_fusion
  144.8 1.6 copy.73
  147.3 11.8 %all-reduce.2 = (bf16[2,128]{1,0:T(2,128)(2,1)S(1)}, bf16[512]{0:T(512)(128)(2,1)S(1)}, bf16[512]{0:T(512)(128)(2,1)S(1)}) all-reduce(bf16[2,128]{1,0:T(2,128)(2,1)S(1)} %bitcast.112, bf16[512]{0:T(512)(128)(2,1)S(1)} %bitcast.110, bf16[512]{0:T(512)(128)(2,1)S(1)} %bitcast.111), channel_id=1, replica_groups=mesh['sp'=4,'dp'=8] {'dp'}, use_global_device_ids=true, to_apply=%region_12.13 | all-reduce | flops 1280 | bytes 5120 | tf_op jit(solution)/shard_map/psum | solution.py:92
  159.2 12.1 %psum.77 = bf16[8,128]{1,0:T(8,128)(2,1)S(1)} all-reduce(bf16[8,128]{1,0:T(8,128)(2,1)S(1)} %dynamic_update_slice.7), channel_id=1, replica_groups=mesh['sp'=4,'dp'=8] {'sp'}, use_global_device_ids=true, to_apply=%region_13.14 | all-reduce | flops 1024 | bytes 4096 | tf_op jit(solution)/shard_map/psum | solution.py:100
  171.3 8.4 %all-reduce = (f32[512]{0:T(512)S(1)}, f32[512]{0:T(512)S(1)}) all-reduce(f32[512]{0:T(512)S(1)} %bitcast.113, f32[512]{0:T(512)S(1)} %bitcast.114), channel_id=1, replica_groups=mesh['sp'=4,'dp'=8] {'sp'}, use_global_device_ids=true, to_apply=%region_7.8 | all-reduce | flops 1024 | bytes 8192 | tf_op jit(solution)/shard_map/psum | solution.py:80
  180.8 2.1 fusion.66
  183.0 1.8 convert_multiply_fusion.9
  184.8 31.6 %reduce-scatter.2.cloned.1.call-done = bf16[256,512]{0,1:T(8,128)(2,1)} async-done(((bf16[2048,512]{0,1:T(8,128)(2,1)}), bf16[256,512]{0,1:T(8,128)(2,1)}) %reduce-scatter.2.cloned.1.call-update) | async-done | bytes 262160 | tf_op jit(solution)/shard_map/reduce_scatter | solution.py:61
  217.3 1.0 copy.83
  (50 shorter events, 10.7 us)
Async XLA Ops:
  7.2 58.4 %all-gather.2.cloned.1.call-start = ((), (), s32[]{:S(2)}) async-start(), calls=%async_computation.2 | async-start | bytes 2359296 | tf_op jit(solution)/shard_map/all_gather | solution.py:49
  10.5 6.6 %copy-start = (bf16[1,512,512]{2,1,0:T(8,128)(2,1)S(1)}, bf16[1,512,512]{2,1,0:T(8,128)(2,1)}, u32[]{:S(2)}) copy-start(bf16[1,512,512]{2,1,0:T(8,128)(2,1)} %param.10) | copy-start | bytes 1572868
  10.5 55.0 %all-to-all-start = ((bf16[4,1,128,2048]{3,2,1,0:T(8,128)(2,1)}), bf16[4,1,128,2048]{3,2,1,0:T(8,128)(2,1)}, u32[]{:S(2)}, u32[]{:S(2)}) async-start(bf16[4,1,128,2048]{3,2,1,0:T(8,128)(2,1)} %stack.2), calls=%async_computation | async-start | bytes 4194304 | tf_op jit(solution)/shard_map/all_to_all | solution.py:51
  17.0 1.3 copy-start.5
  17.0 1.3 copy-start.6
  17.0 1.3 copy-start.2
  17.0 117.8 %all-reduce.6.cloned.1.call-start = ((), (), s32[]{:S(2)}) async-start(), calls=%async_computation.4 | async-start | bytes 131072 | tf_op jit(solution)/shard_map/psum | solution.py:91
  18.3 39.5 %copy-start.7 = (bf16[8,128,128]{2,1,0:T(8,128)(2,1)S(1)}, bf16[8,128,128]{2,1,0:T(8,128)(2,1)}, u32[]{:S(2)}) copy-start(bf16[8,128,128]{2,1,0:T(8,128)(2,1)} %param.12) | copy-start | bytes 786436
  72.3 1.4 copy-start.3
  73.7 109.3 %all-reduce.8.cloned.1.call-start = ((), (), s32[]{:S(2)}) async-start(), calls=%async_computation.5 | async-start | bytes 524288 | tf_op jit(solution)/shard_map/psum | solution.py:99
  135.8 0.7 copy-start.1
  136.5 79.9 %reduce-scatter.2.cloned.1.call-start = ((), (), s32[]{:S(2)}) async-start(), calls=%async_computation.3 | async-start | bytes 2359296 | tf_op jit(solution)/shard_map/reduce_scatter | solution.py:61
  140.9 1.0 copy-start.4
Sparse Core Ops, SparseCore 0:
  9.9 30.4 all-gather.1
  73.8 61.0 all-reduce.5
  137.2 34.9 all-reduce.7
  175.4 40.9 reduce-scatter.1
